TPU v7x, 32 devices: a whole 2x2x4 slice. The times are simulated.
32 devices in a mesh: sp: 8 (over z, y), tp: 4 (over x, core).
Axes of the slice: x: 2, y: 2, z: 4, core: 2. Of those that a mesh axis runs over, the one named last changes fastest.
Arguments:
- tokens: bfloat16 [2048, 2048], P(('sp', 'tp')), may hold values from -6 to 6
- pre_gain: float32 [2048], replicated, may hold values from 0.1 to 1.9
- w_query_ret: bfloat16 [2048, 768], P('sp', 'tp'), may hold values from -0.125 to 0.125
- w_key_ret: bfloat16 [2048, 768], P('sp', 'tp'), may hold values from -0.125 to 0.125
- w_value_ret: bfloat16 [2048, 768], P('sp', 'tp'), may hold values from -0.125 to 0.125
- w_query_att: bfloat16 [2048, 768], P('sp', 'tp'), may hold values from -0.5 to 0.5
- w_key_att: bfloat16 [2048, 256], P('sp', 'tp'), may hold values from -0.125 to 0.125
- w_value_att: bfloat16 [2048, 256], P('sp', 'tp'), may hold values from -0.125 to 0.125
- w_out_ret: bfloat16 [768, 2048], P('tp', 'sp'), may hold values from -0.15625 to 0.15625
- w_out_att: bfloat16 [768, 2048], P('tp', 'sp'), may hold values from -0.15625 to 0.15625
- retain_log: float32 [2048, 12], P('sp', 'tp')
- forget_total: float32 [12, 2048], P('tp'), as said below
Outputs:
- mixed: bfloat16 [2048, 2048], P(('sp', 'tp'))
Inputs may be any that keep to these rules, and one draw needn't show every extreme that they name: `forget_total`: never rises along positions.
All inputs are finite; a program needn't handle non-finite values.
Results may differ from a plain program's by a relative error of at most 0.019.
Values may be sent and summed in bfloat16 or wider, within the bound.
A program may use at most 64 MiB of HBM per device.

v0:
```python
import jax
import jax.numpy as jnp
from jax import lax
from jax.sharding import PartitionSpec as P

HEAD = 64
SPAN = 256
KEY_SPAN = 256
EPS = 1e-06
THETA = 10000.0
HIGH = lax.Precision.HIGHEST


def rotate(field, positions):
    half = field.shape[-1] // 2
    inverse = THETA ** (-jnp.arange(half, dtype=jnp.float32) / half)
    angles = positions[:, None] * inverse[None, :]
    cosine = jnp.cos(angles)[:, None, :]
    sine = jnp.sin(angles)[:, None, :]
    first_half = field[..., :half]
    second_half = field[..., half:]
    return jnp.concatenate(
        [first_half * cosine - second_half * sine, first_half * sine + second_half * cosine],
        axis=-1,
    )


def head_norm(values):
    centre = jnp.mean(values, axis=-1, keepdims=True)
    spread = jnp.mean(jnp.square(values - centre), axis=-1, keepdims=True)
    return (values - centre) * lax.rsqrt(spread + EPS)


def advance(state, pair):
    decay, update = pair
    return (jnp.exp(decay)[:, None, None] * state + update, state)


def body(
    tokens,
    pre_gain,
    w_query_ret,
    w_key_ret,
    w_value_ret,
    w_query_att,
    w_key_att,
    w_value_att,
    w_out_ret,
    w_out_att,
    retain_log,
    forget_total,
):
    rows = tokens.astype(jnp.float32)
    normed = (
        rows * lax.rsqrt(jnp.mean(rows * rows, axis=-1, keepdims=True) + EPS) * pre_gain
    ).astype(jnp.bfloat16)
    gathered = lax.all_gather(normed, "tp", axis=0, tiled=True)
    tok_dev = gathered.shape[0]
    offset = lax.axis_index("sp") * tok_dev
    query_places = offset + jnp.arange(tok_dev, dtype=jnp.int32)
    positions = query_places.astype(jnp.float32)

    def blocked(values):
        return values.reshape((tok_dev // SPAN, SPAN) + values.shape[1:])

    pieces = (
        lax.all_gather(w_query_ret, "sp", axis=0, tiled=True),
        lax.all_gather(w_key_ret, "sp", axis=0, tiled=True),
        lax.all_gather(w_value_ret, "sp", axis=0, tiled=True),
        lax.all_gather(w_query_att, "sp", axis=0, tiled=True),
        lax.all_gather(w_key_att, "sp", axis=0, tiled=True),
        lax.all_gather(w_value_att, "sp", axis=0, tiled=True),
    )
    projected = tuple(
        (jnp.dot(gathered, piece, preferred_element_type=jnp.float32) for piece in pieces)
    )
    heads = retain_log.shape[1]
    shape = (tok_dev, heads, HEAD)
    query = blocked(
        (rotate(projected[0].reshape(shape), positions) * HEAD ** (-0.5)).astype(jnp.bfloat16)
    )
    key_rows = blocked(rotate(projected[1].reshape(shape), positions).astype(jnp.bfloat16))
    value_rows = blocked(projected[2].astype(jnp.bfloat16).reshape(shape))
    within = jnp.cumsum(blocked(retain_log), axis=1)
    causal = jnp.arange(SPAN)[:, None] >= jnp.arange(SPAN)[None, :]
    scores = jnp.einsum("bthd,bshd->bhts", query, key_rows, preferred_element_type=jnp.float32)
    turned = jnp.transpose(within, (0, 2, 1))
    gap = jnp.where(causal, turned[:, :, :, None] - turned[:, :, None, :], 0.0)
    weights = jnp.where(causal, scores * jnp.exp(gap), 0.0).astype(jnp.bfloat16)
    local = jnp.einsum("bhts,bshd->bthd", weights, value_rows, preferred_element_type=jnp.float32)
    last = within[:, -1]
    faded = (key_rows.astype(jnp.float32) * jnp.exp(last[:, None, :] - within)[..., None]).astype(
        jnp.bfloat16
    )
    updates = jnp.einsum("bshd,bshe->bhde", faded, value_rows, preferred_element_type=jnp.float32)
    zero_state = jnp.zeros((heads, HEAD, HEAD), jnp.float32)
    final, _ = lax.scan(advance, zero_state, (last, updates))
    decay_total = jnp.sum(last, axis=0)
    own_state = final.reshape(heads, HEAD * HEAD)
    every_total = lax.all_gather(
        decay_total[None].astype(jnp.bfloat16), "sp", axis=0, tiled=True
    ).astype(jnp.float32)
    every_state = lax.all_gather(
        own_state[None].astype(jnp.bfloat16), "sp", axis=0, tiled=True
    ).astype(jnp.float32)
    device_order = jnp.arange(every_total.shape[0], dtype=jnp.int32)[:, None]
    earlier = device_order < lax.axis_index("sp")
    before = jnp.sum(jnp.where(earlier, every_total, 0.0), axis=0)
    through = jnp.cumsum(every_total, axis=0)
    fading = jnp.where(earlier, jnp.exp(jnp.where(earlier, before[None, :] - through, 0.0)), 0.0)
    incoming = jnp.einsum("jh,jhe->he", fading, every_state, precision=HIGH)
    _, befores = lax.scan(advance, incoming.reshape(heads, HEAD, HEAD), (last, updates))
    lifted = (query.astype(jnp.float32) * jnp.exp(within)[..., None]).astype(jnp.bfloat16)
    carried = jnp.einsum(
        "bthd,bhde->bthe", lifted, befores.astype(jnp.bfloat16), preferred_element_type=jnp.float32
    )
    retained = (
        head_norm((local + carried).reshape(shape))
        .astype(jnp.bfloat16)
        .reshape(tok_dev, heads * HEAD)
    )
    raw_key = projected[4]
    gate_heads = forget_total.shape[0]
    kv_local = raw_key.shape[1] // HEAD
    group = gate_heads // kv_local
    query = (
        (projected[3] * HEAD ** (-0.5)).astype(jnp.bfloat16).reshape(tok_dev, kv_local, group, HEAD)
    )
    key_rows = raw_key.astype(jnp.bfloat16)
    value_rows = projected[5].astype(jnp.bfloat16)
    gate_rows = lax.dynamic_slice_in_dim(forget_total, offset, tok_dev, 1).reshape(
        kv_local, group, tok_dev
    )
    last_row = offset + tok_dev - 1
    init = (
        jnp.zeros((kv_local, group, tok_dev, HEAD), jnp.float32),
        jnp.zeros((kv_local, group, tok_dev), jnp.float32),
    )
    key_piece = lax.all_gather(key_rows, "sp", axis=0, tiled=True)
    value_piece = lax.all_gather(value_rows, "sp", axis=0, tiled=True)
    count = key_piece.shape[0] // KEY_SPAN

    def one_block(index, inner):
        first = index * KEY_SPAN

        def compute(state):
            weighted, total = state
            key_block = lax.dynamic_slice_in_dim(key_piece, index * KEY_SPAN, KEY_SPAN, 0).reshape(
                KEY_SPAN, kv_local, HEAD
            )
            value_block = lax.dynamic_slice_in_dim(
                value_piece, index * KEY_SPAN, KEY_SPAN, 0
            ).reshape(KEY_SPAN, kv_local, HEAD)
            gate_keys = lax.dynamic_slice_in_dim(forget_total, first, KEY_SPAN, 1).reshape(
                kv_local, group, KEY_SPAN
            )
            scores = jnp.einsum(
                "tcgd,scd->cgts", query, key_block, preferred_element_type=jnp.float32
            )
            logits = scores + gate_rows[:, :, :, None] - gate_keys[:, :, None, :]
            allowed = (first + jnp.arange(KEY_SPAN, dtype=jnp.int32))[None, :] <= query_places[
                :, None
            ]
            weights = jnp.exp(jnp.where(allowed, logits, -jnp.inf))
            total = total + jnp.sum(weights, axis=-1)
            weighted = weighted + jnp.einsum(
                "cgts,scd->cgtd",
                weights.astype(jnp.bfloat16),
                value_block,
                preferred_element_type=jnp.float32,
            )
            return (weighted, total)

        def skipped(state):
            return state

        return lax.cond(first <= last_row, compute, skipped, inner)

    weighted, total = lax.fori_loop(0, count, one_block, init)
    result = weighted / total[..., None]
    attended = (
        jnp.transpose(result, (2, 0, 1, 3)).reshape(tok_dev, gate_heads * HEAD).astype(jnp.bfloat16)
    )
    out_ret, out_att = (
        lax.all_gather(w_out_ret, "sp", axis=1, tiled=True),
        lax.all_gather(w_out_att, "sp", axis=1, tiled=True),
    )
    return lax.psum_scatter(
        (
            jnp.dot(retained, out_ret, preferred_element_type=jnp.float32)
            + jnp.dot(attended, out_att, preferred_element_type=jnp.float32)
        ).astype(jnp.bfloat16),
        "tp",
        scatter_dimension=0,
        tiled=True,
    )


def solution(mesh):
    return jax.shard_map(
        body,
        mesh=mesh,
        in_specs=(
            P(("sp", "tp"), None),
            P(),
            P("sp", "tp"),
            P("sp", "tp"),
            P("sp", "tp"),
            P("sp", "tp"),
            P("sp", "tp"),
            P("sp", "tp"),
            P("tp", "sp"),
            P("tp", "sp"),
            P("sp", "tp"),
            P("tp", None),
        ),
        out_specs=P(("sp", "tp"), None),
        check_vma=False,
    )
```

profile of v0, /device:TPU:0, one launch (start us, length us, event | category | flops | bytes accessed | tf_op | source)
XLA Modules:
  0.0 463.0 jit_solution(11235559087776837710)
XLA Ops:
  6.5 0.0 all-gather.3.cloned.1.call-start
  6.6 1.2 fusion.24
  7.8 1.8 fusion.26
  9.6 0.0 all-gather.3.cloned.1.call-update
  9.6 0.0 reduce-scatter.2.cloned.1.call-start
  9.7 0.7 reshape.332
  10.4 0.9 reduce-window.6
  11.3 0.1 slice.32
  11.4 0.1 copy.39
  11.5 0.1 copy.41
  11.7 0.0 copy-start.6
  11.7 22.4 %all-gather = bf16[8,1,3]{2,1,0:T(2,128)(2,1)S(1)} all-gather(bf16[1,1,3]{2,1,0:T(2,128)(2,1)S(1)} %slice.47), channel_id=2, replica_groups=mesh['sp'=8,'tp'=4] {'sp'}, dimensions={0}, use_global_device_ids=true | all-gather | bytes 54 | tf_op jit(solution)/shard_map/all_gather | solution.py:100
  34.2 0.1 copy.42
  34.3 0.1 copy.40
  34.4 0.6 bitcast_add_fusion.2
  35.0 0.1 copy.44
  35.1 0.2 reduce_window_sum.43
  35.3 0.1 copy.43
  35.4 0.0 copy-done.9
  35.4 32.9 %all_gather.46 = bf16[2048,64]{0,1:T(8,128)(2,1)} all-gather(bf16[256,64]{0,1:T(8,128)(2,1)S(1)} %copy-done.9), channel_id=1, replica_groups=mesh['sp'=8,'tp'=4] {'sp'}, dimensions={0}, use_global_device_ids=true | all-gather | bytes 294912 | tf_op jit(solution)/shard_map/all_gather | solution.py:71
  68.3 0.0 copy-done.10
  68.3 33.0 %all_gather.49 = bf16[2048,64]{0,1:T(8,128)(2,1)} all-gather(bf16[256,64]{0,1:T(8,128)(2,1)S(1)} %copy-done.10), channel_id=1, replica_groups=mesh['sp'=8,'tp'=4] {'sp'}, dimensions={0}, use_global_device_ids=true | all-gather | bytes 294912 | tf_op jit(solution)/shard_map/all_gather | solution.py:72
  101.3 0.0 copy-done.3
  101.3 34.4 %all_gather.41 = bf16[2048,192]{0,1:T(8,128)(2,1)} all-gather(bf16[256,192]{0,1:T(8,128)(2,1)S(1)} %copy-done.3), channel_id=1, replica_groups=mesh['sp'=8,'tp'=4] {'sp'}, dimensions={0}, use_global_device_ids=true | all-gather | bytes 884736 | tf_op jit(solution)/shard_map/all_gather | solution.py:67
  135.7 31.8 %all_gather.42 = bf16[2048,192]{0,1:T(8,128)(2,1)S(1)} all-gather(bf16[256,192]{0,1:T(8,128)(2,1)S(1)} %copy-done.4), channel_id=1, replica_groups=mesh['sp'=8,'tp'=4] {'sp'}, dimensions={0}, use_global_device_ids=true | all-gather | bytes 884736 | tf_op jit(solution)/shard_map/all_gather | solution.py:68
  167.5 0.7 constant_dynamic-slice_fusion.1
  168.2 0.2 multiply_cosine_fusion
  168.4 0.1 select_reduce_fusion
  168.5 0.1 select_bitcast_fusion
  168.6 0.6 exponential_multiply_fusion
  169.2 34.6 %all_gather.40 = bf16[2048,192]{0,1:T(8,128)(2,1)} all-gather(bf16[256,192]{0,1:T(8,128)(2,1)S(1)} %copy-done.5), channel_id=1, replica_groups=mesh['sp'=8,'tp'=4] {'sp'}, dimensions={0}, use_global_device_ids=true | all-gather | bytes 884736 | tf_op jit(solution)/shard_map/all_gather | solution.py:69
  203.7 32.4 %all_gather.48 = bf16[2048,192]{0,1:T(8,128)(2,1)S(1)} all-gather(bf16[256,192]{0,1:T(8,128)(2,1)S(1)} %copy-done.6), channel_id=1, replica_groups=mesh['sp'=8,'tp'=4] {'sp'}, dimensions={0}, use_global_device_ids=true | all-gather | bytes 884736 | tf_op jit(solution)/shard_map/all_gather | solution.py:70
  236.1 32.2 %all_gather.45 = bf16[192,2048]{1,0:T(8,128)(2,1)S(1)} all-gather(bf16[192,256]{1,0:T(8,128)(2,1)S(1)} %copy-done.7), channel_id=1, replica_groups=mesh['sp'=8,'tp'=4] {'sp'}, dimensions={1}, use_global_device_ids=true | all-gather | bytes 884736 | tf_op jit(solution)/shard_map/all_gather | solution.py:185
  268.3 0.0 copy-done.8
  268.3 33.8 %all_gather.51 = bf16[192,2048]{1,0:T(8,128)(2,1)} all-gather(bf16[192,256]{1,0:T(8,128)(2,1)S(1)} %copy-done.8), channel_id=1, replica_groups=mesh['sp'=8,'tp'=4] {'sp'}, dimensions={1}, use_global_device_ids=true | all-gather | bytes 884736 | tf_op jit(solution)/shard_map/all_gather | solution.py:186
  302.1 1.8 convolution_convert_fusion.2
  303.9 32.8 %all_gather.47 = bf16[2048,64]{0,1:T(8,128)(2,1)} all-gather(bf16[256,64]{0,1:T(8,128)(2,1)S(1)} %convolution_convert_fusion.2), channel_id=1, replica_groups=mesh['sp'=8,'tp'=4] {'sp'}, dimensions={0}, use_global_device_ids=true | all-gather | bytes 294912 | tf_op jit(solution)/shard_map/all_gather | solution.py:139
  336.7 1.7 convolution_convert_fusion.1
  338.4 32.7 %all_gather.50 = bf16[2048,64]{0,1:T(8,128)(2,1)} all-gather(bf16[256,64]{0,1:T(8,128)(2,1)S(1)} %convolution_convert_fusion.1), channel_id=1, replica_groups=mesh['sp'=8,'tp'=4] {'sp'}, dimensions={0}, use_global_device_ids=true | all-gather | bytes 294912 | tf_op jit(solution)/shard_map/all_gather | solution.py:140
  371.2 1.7 fusion.56
  372.9 0.5 fusion.57
  373.4 0.1 multiply_subtract_fusion
  373.5 0.0 copy-done.1
  373.5 0.5 convolution_convert_fusion
  374.0 0.1 fusion.38
  374.2 0.1 squeeze.16
  374.3 0.1 add_convert_fusion.1
  374.4 30.7 %all_gather.44 = bf16[8,3,4096]{2,1,0:T(4,128)(2,1)S(1)} all-gather(bf16[1,3,4096]{2,1,0:T(4,128)(2,1)S(1)} %add_convert_fusion.1), channel_id=1, replica_groups=mesh['sp'=8,'tp'=4] {'sp'}, dimensions={0}, use_global_device_ids=true | all-gather | bytes 221184 | tf_op jit(solution)/shard_map/all_gather | solution.py:103
  405.1 0.5 fusion.36
  405.7 0.1 convert_element_type.142
  405.8 0.5 fusion.19
  406.3 0.2 bitcast_reduce_fusion
  406.6 0.5 fusion.20
  407.2 3.4 while.10
  407.2 3.0 conditional.3
  407.2 0.7 constant_dynamic-slice_fusion
  407.9 0.1 broadcast_compare_fusion
  408.0 1.2 fusion.55
  409.2 1.0 fusion.6
  410.6 0.5 fusion.58
  411.1 0.6 copy-done.2
  411.7 1.4 fusion.16
  413.2 0.0 reduce-scatter.2.cloned.1.call-update
  413.2 42.9 %reduce-scatter.2.cloned.1.call-done = bf16[64,2048]{1,0:T(8,128)(2,1)} async-done(((bf16[256,2048]{1,0:T(8,128)(2,1)}), bf16[64,2048]{1,0:T(8,128)(2,1)}) %reduce-scatter.2.cloned.1.call-update) | async-done | bytes 262160 | tf_op jit(solution)/shard_map/reduce_scatter | solution.py:188
  (59 shorter events, 0.5 us)
Async XLA Ops:
  6.5 28.8 %copy-start.9 = (bf16[256,64]{0,1:T(8,128)(2,1)S(1)}, bf16[256,64]{0,1:T(8,128)(2,1)}, u32[]{:S(2)}) copy-start(bf16[256,64]{0,1:T(8,128)(2,1)} %param.22) | copy-start | bytes 98308
  6.5 61.7 %copy-start.10 = (bf16[256,64]{0,1:T(8,128)(2,1)S(1)}, bf16[256,64]{0,1:T(8,128)(2,1)}, u32[]{:S(2)}) copy-start(bf16[256,64]{0,1:T(8,128)(2,1)} %param.23) | copy-start | bytes 98308
  6.5 94.8 %copy-start.3 = (bf16[256,192]{0,1:T(8,128)(2,1)S(1)}, bf16[256,192]{0,1:T(8,128)(2,1)}, u32[]{:S(2)}) copy-start(bf16[256,192]{0,1:T(8,128)(2,1)} %param.18) | copy-start | bytes 294916
  6.5 129.2 %copy-start.4 = (bf16[256,192]{0,1:T(8,128)(2,1)S(1)}, bf16[256,192]{0,1:T(8,128)(2,1)}, u32[]{:S(2)}) copy-start(bf16[256,192]{0,1:T(8,128)(2,1)} %param.19) | copy-start | bytes 294916
  6.5 295.6 %all-gather.3.cloned.1.call-start = ((), (), s32[]{:S(2)}) async-start(), calls=%async_computation.1 | async-start | bytes 1310720 | tf_op jit(solution)/shard_map/all_gather | solution.py:57
  9.6 159.6 %copy-start.5 = (bf16[256,192]{0,1:T(8,128)(2,1)S(1)}, bf16[256,192]{0,1:T(8,128)(2,1)}, u32[]{:S(2)}) copy-start(bf16[256,192]{0,1:T(8,128)(2,1)} %param.20) | copy-start | bytes 294916
  9.6 446.5 %reduce-scatter.2.cloned.1.call-start = ((), (), s32[]{:S(2)}) async-start(), calls=%async_computation.2 | async-start | bytes 1310720 | tf_op jit(solution)/shard_map/reduce_scatter | solution.py:188
  11.7 192.0 %copy-start.6 = (bf16[256,192]{0,1:T(8,128)(2,1)S(1)}, bf16[256,192]{0,1:T(8,128)(2,1)}, u32[]{:S(2)}) copy-start(bf16[256,192]{0,1:T(8,128)(2,1)} %param.21) | copy-start | bytes 294916
  35.4 200.7 %copy-start.7 = (bf16[192,256]{1,0:T(8,128)(2,1)S(1)}, bf16[192,256]{1,0:T(8,128)(2,1)}, u32[]{:S(2)}) copy-start(bf16[192,256]{1,0:T(8,128)(2,1)} %param.24) | copy-start | bytes 294916
  101.3 167.0 %copy-start.8 = (bf16[192,256]{1,0:T(8,128)(2,1)S(1)}, bf16[192,256]{1,0:T(8,128)(2,1)}, u32[]{:S(2)}) copy-start(bf16[192,256]{1,0:T(8,128)(2,1)} %param.25) | copy-start | bytes 294916
  302.1 69.1 %copy-start = (bf16[256,2048]{1,0:T(8,128)(2,1)S(1)}, bf16[256,2048]{1,0:T(8,128)(2,1)}, u32[]{:S(2)}) copy-start(bf16[256,2048]{1,0:T(8,128)(2,1)} %all-gather.3.cloned.1.call-done) | copy-start | bytes 3145732
  371.2 2.3 copy-start.1
  373.4 0.9 copy-start.12
  373.4 32.3 %copy-start.11 = (f32[3,256]{1,0:T(4,128)S(1)}, f32[3,256]{1,0:T(4,128)}, u32[]{:S(2)}) copy-start(f32[3,256]{1,0:T(4,128)} %bitcast_add_fusion.2) | copy-start | bytes 9220
  410.6 1.1 copy-start.2
Sparse Core Ops, SparseCore 0:
  9.7 19.4 all-gather.2
  413.3 42.7 reduce-scatter.1
where the time goes:
time: 465 us; the launch traced here: 463 us
  blocking collectives  384 us (83%)
  waiting for transfers between devices  43 us (9%)
  between operations  13.7 us (3%)
  matrix products  12.1 us (3%)
  other arithmetic  6.14 us (1%)
    reduce_scatter x1, waiting for transfers between devices, body(): lax.psum_scatter((jnp.dot(retained, out_ret, preferred_element_type=jnp.f...  42.9 us
    all_gather x1, blocking collectives, body(): lax.all_gather(w_value_ret, 'sp', axis=0, tiled=True)  34.6 us
    all_gather x1, blocking collectives, body(): lax.all_gather(w_query_ret, 'sp', axis=0, tiled=True)  34.4 us
    all_gather x1, blocking collectives, body(): lax.all_gather(w_out_att, 'sp', axis=1, tiled=True)  33.8 us
    all_gather x1, blocking collectives, body(): lax.all_gather(w_value_att, 'sp', axis=0, tiled=True)  33 us
    all_gather x1, blocking collectives, body(): lax.all_gather(w_key_att, 'sp', axis=0, tiled=True)  32.9 us
    all_gather x1, blocking collectives, body(): key_piece = lax.all_gather(key_rows, 'sp', axis=0, tiled=True)  32.8 us
    all_gather x1, blocking collectives, body(): value_piece = lax.all_gather(value_rows, 'sp', axis=0, tiled=True)  32.7 us
  transfers between devices with their start and end apart: 2, of which 1 were waited for; matrix products, arithmetic and copies ran while one was open for 1% of the time, Pallas kernels for 0%

commit v1 on v0

--- a/solution.py
+++ b/solution.py
@@ -137,7 +137,9 @@
         jnp.zeros((kv_local, group, tok_dev), jnp.float32),
     )
     key_piece = lax.all_gather(key_rows, "sp", axis=0, tiled=True)
-    value_piece = lax.all_gather(value_rows, "sp", axis=0, tiled=True)
+    value_piece = jnp.concatenate(
+        lax.all_to_all(jnp.stack([value_rows] * lax.axis_size("sp")), "sp", 0, 0), axis=0
+    )
     count = key_piece.shape[0] // KEY_SPAN
 
     def one_block(index, inner):

time: 465 us -> 437 us (0.940)
  blocking collectives: 384 us -> 350 us
    all_gather x1 -> x0, blocking collectives: 32.7 us -> none  [body(): value_piece = lax.all_gather(value_rows, 'sp', axis=0, tiled=True)]
  transfers between devices with their start and end apart: 2 -> 3, of which waited for: 1 -> 1; matrix products, arithmetic and copies ran while one was open for 1% -> 4% of each run, Pallas kernels for 0% -> 0%
where the time goes in v1:
time: 437 us; the launch traced here: 436 us
  blocking collectives  350 us (80%)
  waiting for transfers between devices  41.5 us (9%)
  matrix products  13.8 us (3%)
  between operations  13.7 us (3%)
  other arithmetic  8.73 us (2%)
    reduce_scatter x1, waiting for transfers between devices, body(): lax.psum_scatter((jnp.dot(retained, out_ret, preferred_element_type=jnp.f...  41.5 us
    all_gather x1, blocking collectives, body(): lax.all_gather(w_value_ret, 'sp', axis=0, tiled=True)  34.7 us
    all_gather x1, blocking collectives, body(): lax.all_gather(w_query_ret, 'sp', axis=0, tiled=True)  34.6 us
    all_gather x1, blocking collectives, body(): lax.all_gather(w_key_ret, 'sp', axis=0, tiled=True)  34 us
    all_gather x1, blocking collectives, body(): lax.all_gather(w_out_att, 'sp', axis=1, tiled=True)  34 us
    all_gather x1, blocking collectives, body(): key_piece = lax.all_gather(key_rows, 'sp', axis=0, tiled=True)  32.7 us
    all_gather x1, blocking collectives, body(): lax.all_gather(w_query_att, 'sp', axis=0, tiled=True)  32.3 us
    all_gather x1, blocking collectives, body(): lax.all_gather(w_out_ret, 'sp', axis=1, tiled=True)  32.2 us
  transfers between devices with their start and end apart: 3, of which 1 were waited for; matrix products, arithmetic and copies ran while one was open for 4% of the time, Pallas kernels for 0%

profile of v1, /device:TPU:0, one launch (start us, length us, event | category | flops | bytes accessed | tf_op | source)
XLA Modules:
  0.0 435.9 jit_solution(9281071471277855378)
XLA Ops:
  6.5 0.0 all-gather.3.cloned.1.call-start
  6.6 1.2 fusion.24
  7.8 1.8 fusion.26
  9.6 0.0 all-gather.3.cloned.1.call-update
  9.6 0.7 iota_compare_fusion
  10.3 0.7 reshape.337
  11.0 0.9 reduce-window.6
  11.9 0.1 slice.32
  11.9 0.1 copy.47
  12.1 0.1 copy.49
  12.3 0.0 copy-start.7
  12.3 22.4 %all-gather = bf16[8,1,3]{2,1,0:T(2,128)(2,1)S(1)} all-gather(bf16[1,1,3]{2,1,0:T(2,128)(2,1)S(1)} %slice.47), channel_id=2, replica_groups=mesh['sp'=8,'tp'=4] {'sp'}, dimensions={0}, use_global_device_ids=true | all-gather | bytes 54 | tf_op jit(solution)/shard_map/all_gather | solution.py:100
  34.7 0.1 copy.50
  34.9 0.1 copy.48
  35.0 0.6 bitcast_add_fusion.2
  35.6 0.1 copy.52
  35.6 0.2 reduce_window_sum.43
  35.9 0.1 copy.51
  36.0 30.9 %all_gather.43 = bf16[2048,64]{0,1:T(8,128)(2,1)S(1)} all-gather(bf16[256,64]{0,1:T(8,128)(2,1)S(1)} %copy-done.13), channel_id=1, replica_groups=mesh['sp'=8,'tp'=4] {'sp'}, dimensions={0}, use_global_device_ids=true | all-gather | bytes 294912 | tf_op jit(solution)/shard_map/all_gather | solution.py:71
  66.8 30.9 %all_gather.46 = bf16[2048,64]{0,1:T(8,128)(2,1)S(1)} all-gather(bf16[256,64]{0,1:T(8,128)(2,1)S(1)} %copy-done.14), channel_id=1, replica_groups=mesh['sp'=8,'tp'=4] {'sp'}, dimensions={0}, use_global_device_ids=true | all-gather | bytes 294912 | tf_op jit(solution)/shard_map/all_gather | solution.py:72
  97.7 34.6 %all_gather.38 = bf16[2048,192]{0,1:T(8,128)(2,1)} all-gather(bf16[256,192]{0,1:T(8,128)(2,1)S(1)} %copy-done.4), channel_id=1, replica_groups=mesh['sp'=8,'tp'=4] {'sp'}, dimensions={0}, use_global_device_ids=true | all-gather | bytes 884736 | tf_op jit(solution)/shard_map/all_gather | solution.py:67
  132.3 34.0 %all_gather.39 = bf16[2048,192]{0,1:T(8,128)(2,1)} all-gather(bf16[256,192]{0,1:T(8,128)(2,1)S(1)} %copy-done.5), channel_id=1, replica_groups=mesh['sp'=8,'tp'=4] {'sp'}, dimensions={0}, use_global_device_ids=true | all-gather | bytes 884736 | tf_op jit(solution)/shard_map/all_gather | solution.py:68
  166.4 0.7 constant_dynamic-slice_fusion.1
  167.0 0.8 multiply_cosine_fusion
  167.9 0.1 select_reduce_fusion
  168.0 0.1 select_bitcast_fusion
  168.0 0.6 exponential_multiply_fusion
  168.7 34.7 %all_gather.37 = bf16[2048,192]{0,1:T(8,128)(2,1)} all-gather(bf16[256,192]{0,1:T(8,128)(2,1)S(1)} %copy-done.6), channel_id=1, replica_groups=mesh['sp'=8,'tp'=4] {'sp'}, dimensions={0}, use_global_device_ids=true | all-gather | bytes 884736 | tf_op jit(solution)/shard_map/all_gather | solution.py:69
  203.3 32.3 %all_gather.45 = bf16[2048,192]{0,1:T(8,128)(2,1)S(1)} all-gather(bf16[256,192]{0,1:T(8,128)(2,1)S(1)} %copy-done.7), channel_id=1, replica_groups=mesh['sp'=8,'tp'=4] {'sp'}, dimensions={0}, use_global_device_ids=true | all-gather | bytes 884736 | tf_op jit(solution)/shard_map/all_gather | solution.py:70
  235.7 32.2 %all_gather.42 = bf16[192,2048]{1,0:T(8,128)(2,1)S(1)} all-gather(bf16[192,256]{1,0:T(8,128)(2,1)S(1)} %copy-done.8), channel_id=1, replica_groups=mesh['sp'=8,'tp'=4] {'sp'}, dimensions={1}, use_global_device_ids=true | all-gather | bytes 884736 | tf_op jit(solution)/shard_map/all_gather | solution.py:187
  267.8 34.0 %all_gather.47 = bf16[192,2048]{1,0:T(8,128)(2,1)} all-gather(bf16[192,256]{1,0:T(8,128)(2,1)S(1)} %copy-done.9), channel_id=1, replica_groups=mesh['sp'=8,'tp'=4] {'sp'}, dimensions={1}, use_global_device_ids=true | all-gather | bytes 884736 | tf_op jit(solution)/shard_map/all_gather | solution.py:188
  301.8 1.8 convolution_convert_fusion.1
  303.6 0.7 stack.2
  304.3 3.4 all-to-all-start
  307.7 0.0 reduce-scatter.2.cloned.1.call-start
  307.8 1.7 fusion.56
  309.5 1.6 fusion.57
  311.1 0.7 multiply_subtract_fusion
  311.8 0.5 convolution_convert_fusion
  312.4 0.1 copy-done.11
  312.5 0.0 copy-done.12
  312.5 0.1 fusion.38
  312.6 0.1 squeeze.16
  312.8 0.3 copy-done.10
  313.0 0.8 add_convert_fusion.1
  313.8 31.2 %all_gather.41 = bf16[8,3,4096]{2,1,0:T(4,128)(2,1)S(1)} all-gather(bf16[1,3,4096]{2,1,0:T(4,128)(2,1)S(1)} %add_convert_fusion.1), channel_id=1, replica_groups=mesh['sp'=8,'tp'=4] {'sp'}, dimensions={0}, use_global_device_ids=true | all-gather | bytes 221184 | tf_op jit(solution)/shard_map/all_gather | solution.py:103
  345.0 0.5 fusion.36
  345.5 0.1 convert_element_type.142
  345.6 2.2 fusion.19
  347.7 1.2 bitcast_reduce_fusion
  349.0 0.4 convolution_convert_fusion.2
  349.4 0.5 fusion.20
  350.0 32.7 %all_gather.44 = bf16[2048,64]{0,1:T(8,128)(2,1)} all-gather(bf16[256,64]{0,1:T(8,128)(2,1)S(1)} %convolution_convert_fusion.2), channel_id=1, replica_groups=mesh['sp'=8,'tp'=4] {'sp'}, dimensions={0}, use_global_device_ids=true | all-gather | bytes 294912 | tf_op jit(solution)/shard_map/all_gather | solution.py:139
  382.7 0.5 fusion.58
  383.2 0.0 all-to-all-done
  383.3 2.7 while.10
  383.3 2.3 conditional.3
  383.4 0.8 constant_dynamic-slice_fusion
  384.1 0.1 broadcast_compare_fusion
  384.2 1.2 fusion.55
  385.4 0.2 fusion.6
  386.1 1.4 fusion.16
  387.5 0.0 reduce-scatter.2.cloned.1.call-update
  387.5 41.5 %reduce-scatter.2.cloned.1.call-done = bf16[64,2048]{1,0:T(8,128)(2,1)} async-done(((bf16[256,2048]{1,0:T(8,128)(2,1)}), bf16[64,2048]{1,0:T(8,128)(2,1)}) %reduce-scatter.2.cloned.1.call-update) | async-done | bytes 262160 | tf_op jit(solution)/shard_map/reduce_scatter | solution.py:190
  (66 shorter events, 0.5 us)
Async XLA Ops:
  6.5 29.4 %copy-start.13 = (bf16[256,64]{0,1:T(8,128)(2,1)S(1)}, bf16[256,64]{0,1:T(8,128)(2,1)}, u32[]{:S(2)}) copy-start(bf16[256,64]{0,1:T(8,128)(2,1)} %param.22) | copy-start | bytes 98308
  6.5 60.3 %copy-start.14 = (bf16[256,64]{0,1:T(8,128)(2,1)S(1)}, bf16[256,64]{0,1:T(8,128)(2,1)}, u32[]{:S(2)}) copy-start(bf16[256,64]{0,1:T(8,128)(2,1)} %param.23) | copy-start | bytes 98308
  6.5 91.2 %copy-start.4 = (bf16[256,192]{0,1:T(8,128)(2,1)S(1)}, bf16[256,192]{0,1:T(8,128)(2,1)}, u32[]{:S(2)}) copy-start(bf16[256,192]{0,1:T(8,128)(2,1)} %param.18) | copy-start | bytes 294916
  6.5 125.8 %copy-start.5 = (bf16[256,192]{0,1:T(8,128)(2,1)S(1)}, bf16[256,192]{0,1:T(8,128)(2,1)}, u32[]{:S(2)}) copy-start(bf16[256,192]{0,1:T(8,128)(2,1)} %param.19) | copy-start | bytes 294916
  6.5 295.2 %all-gather.3.cloned.1.call-start = ((), (), s32[]{:S(2)}) async-start(), calls=%async_computation.2 | async-start | bytes 1310720 | tf_op jit(solution)/shard_map/all_gather | solution.py:57
  9.6 159.1 %copy-start.6 = (bf16[256,192]{0,1:T(8,128)(2,1)S(1)}, bf16[256,192]{0,1:T(8,128)(2,1)}, u32[]{:S(2)}) copy-start(bf16[256,192]{0,1:T(8,128)(2,1)} %param.20) | copy-start | bytes 294916
  12.3 191.1 %copy-start.7 = (bf16[256,192]{0,1:T(8,128)(2,1)S(1)}, bf16[256,192]{0,1:T(8,128)(2,1)}, u32[]{:S(2)}) copy-start(bf16[256,192]{0,1:T(8,128)(2,1)} %param.21) | copy-start | bytes 294916
  36.0 199.7 %copy-start.8 = (bf16[192,256]{1,0:T(8,128)(2,1)S(1)}, bf16[192,256]{1,0:T(8,128)(2,1)}, u32[]{:S(2)}) copy-start(bf16[192,256]{1,0:T(8,128)(2,1)} %param.24) | copy-start | bytes 294916
  97.7 170.1 %copy-start.9 = (bf16[192,256]{1,0:T(8,128)(2,1)S(1)}, bf16[192,256]{1,0:T(8,128)(2,1)}, u32[]{:S(2)}) copy-start(bf16[192,256]{1,0:T(8,128)(2,1)} %param.25) | copy-start | bytes 294916
  301.8 6.0 %copy-start = (bf16[256,2048]{1,0:T(8,128)(2,1)S(1)}, bf16[256,2048]{1,0:T(8,128)(2,1)}, u32[]{:S(2)}) copy-start(bf16[256,2048]{1,0:T(8,128)(2,1)} %all-gather.3.cloned.1.call-done) | copy-start | bytes 3145732
  304.3 78.9 %all-to-all-start = ((bf16[8,256,64]{1,2,0:T(8,128)(2,1)}), bf16[8,256,64]{1,2,0:T(8,128)(2,1)S(1)}, u32[]{:S(2)}, u32[]{:S(2)}) async-start(bf16[8,256,64]{1,2,0:T(8,128)(2,1)} %stack.2), calls=%async_computation | async-start | bytes 524288 | tf_op jit(solution)/shard_map/all_to_all | solution.py:141
  307.7 3.4 copy-start.3
  307.7 121.3 %reduce-scatter.2.cloned.1.call-start = ((), (), s32[]{:S(2)}) async-start(), calls=%async_computation.3 | async-start | bytes 1310720 | tf_op jit(solution)/shard_map/reduce_scatter | solution.py:190
  307.8 4.1 copy-start.1
  311.8 0.6 copy-start.11
  311.8 0.6 copy-start.12
  312.4 0.6 copy-start.10
  383.3 2.8 copy-start.2
Sparse Core Ops, SparseCore 0:
  9.7 19.4 all-gather.2
  387.6 41.3 reduce-scatter.1
